TPU v7x, 32 devices: a whole 2x2x4 slice. The times are simulated.
32 devices in a mesh: fs: 8 (over z, y), tp: 4 (over x, core).
Axes of the slice: x: 2, y: 2, z: 4, core: 2. Of those that a mesh axis runs over, the one named last changes fastest.
Arguments:
- tokens: bfloat16 [640, 3072], P('tp'), may hold values from -6 to 6
- gain_first: float32 [3072], replicated, may hold values from 0.1 to 1.9
- gain_second: float32 [3072], replicated, may hold values from 0.1 to 1.9
- gate_first: float32 [3072, 8192], P('fs', 'tp'), may hold values from -0.109375 to 0.109375
- up_first: float32 [3072, 8192], P('fs', 'tp'), may hold values from -0.109375 to 0.109375
- down_first: float32 [8192, 3072], P('fs', 'tp'), may hold values from -0.09375 to 0.09375
- gate_second: float32 [3072, 8192], P('fs', 'tp'), may hold values from -0.109375 to 0.109375
- up_second: float32 [3072, 8192], P('fs', 'tp'), may hold values from -0.109375 to 0.109375
- down_second: float32 [8192, 3072], P('fs', 'tp'), may hold values from -0.09375 to 0.09375
Outputs:
- result_rows: bfloat16 [640, 3072], P('tp')
- serve_gate_first: bfloat16 [3072, 8192], P(None, 'fs')
- serve_up_first: bfloat16 [3072, 8192], P(None, 'fs')
- serve_down_first: bfloat16 [8192, 3072], P('fs')
- serve_gate_second: bfloat16 [3072, 8192], P(None, 'fs')
- serve_up_second: bfloat16 [3072, 8192], P(None, 'fs')
- serve_down_second: bfloat16 [8192, 3072], P('fs')
All inputs are finite; a program needn't handle non-finite values.
Results may differ from a plain program's by a relative error of at most 0.011.
Values may be sent and summed in bfloat16 or wider, within the bound.
A program may use at most 192 MiB of HBM per device.

v0:
```python
import jax
import jax.numpy as jnp
from jax import lax
from jax.sharding import PartitionSpec as P


def plain_norm(values):
    values = values.astype(jnp.float32)
    center = jnp.mean(values, axis=-1, keepdims=True)
    spread = jnp.mean(jnp.square(values - center), axis=-1, keepdims=True)
    return (values - center) * lax.rsqrt(spread + 1e-05)


def half_step(normed, scales, w_gate, w_rising, w_down):
    gate_part = jnp.dot(normed, w_gate, preferred_element_type=jnp.float32)
    rising = jnp.dot(normed, w_rising, preferred_element_type=jnp.float32)
    hidden = (jax.nn.silu(gate_part) * rising).astype(jnp.bfloat16)
    partial_value = jnp.dot(hidden, w_down, preferred_element_type=jnp.float32)
    block = lax.psum(partial_value, "fs")
    mixed = 1.6817928 * scales[None, :] * normed.astype(jnp.float32) + 0.5 * block
    return plain_norm(mixed).astype(jnp.bfloat16)


def on_device(
    tokens,
    gain_first,
    gain_second,
    gate_first,
    up_first,
    down_first,
    gate_second,
    up_second,
    down_second,
):
    row_count = gate_first.shape[0]
    offset = lax.axis_index("fs") * row_count

    def fold_gain(weight, scales):
        picked = lax.dynamic_slice_in_dim(scales, offset, row_count, 0)
        return (picked[:, None] * weight).astype(jnp.bfloat16)

    widened = (
        lax.all_gather(fold_gain(gate_first, gain_first), "tp", axis=1, tiled=True),
        lax.all_gather(fold_gain(up_first, gain_first), "tp", axis=1, tiled=True),
        lax.all_gather(fold_gain(gate_second, gain_second), "tp", axis=1, tiled=True),
        lax.all_gather(fold_gain(up_second, gain_second), "tp", axis=1, tiled=True),
        lax.all_gather(down_first.astype(jnp.bfloat16), "tp", axis=1, tiled=True),
        lax.all_gather(down_second.astype(jnp.bfloat16), "tp", axis=1, tiled=True),
    )
    regrouped = (
        lax.all_to_all(widened[0], "fs", split_axis=1, concat_axis=0, tiled=True),
        lax.all_to_all(widened[1], "fs", split_axis=1, concat_axis=0, tiled=True),
        lax.all_to_all(widened[2], "fs", split_axis=1, concat_axis=0, tiled=True),
        lax.all_to_all(widened[3], "fs", split_axis=1, concat_axis=0, tiled=True),
    )
    serve_gate_first, serve_up_first, serve_gate_second, serve_up_second = regrouped
    serve_down_first = widened[4]
    serve_down_second = widened[5]
    normed_zero = plain_norm(tokens).astype(jnp.bfloat16)
    normed_one = half_step(
        normed_zero, gain_first, serve_gate_first, serve_up_first, serve_down_first
    )
    result_rows = half_step(
        normed_one, gain_second, serve_gate_second, serve_up_second, serve_down_second
    )
    return (
        result_rows,
        serve_gate_first,
        serve_up_first,
        serve_down_first,
        serve_gate_second,
        serve_up_second,
        serve_down_second,
    )


def solution(mesh):
    placed = (
        P("tp", None),
        P(),
        P(),
        P("fs", "tp"),
        P("fs", "tp"),
        P("fs", "tp"),
        P("fs", "tp"),
        P("fs", "tp"),
        P("fs", "tp"),
    )
    return jax.shard_map(
        on_device,
        mesh=mesh,
        in_specs=placed,
        out_specs=(
            P("tp", None),
            P(None, "fs"),
            P(None, "fs"),
            P("fs", None),
            P(None, "fs"),
            P(None, "fs"),
            P("fs", None),
        ),
        check_vma=False,
    )
```

profile of v0, /device:TPU:0, one launch (start us, length us, event | category | flops | bytes accessed | tf_op | source)
XLA Modules:
  0.0 865.7 jit_solution(17595812001735718184)
XLA Ops:
  8.0 5.5 multiply_convert_fusion.3
  14.3 48.5 %all-gather.7.cloned.1.call-done = bf16[384,8192]{1,0:T(8,128)(2,1)} async-done(((bf16[384,2048]{1,0:T(8,128)(2,1)}), bf16[384,8192]{1,0:T(8,128)(2,1)}) %all-gather.7.cloned.1.call-update) | async-done | bytes 6291472 | tf_op jit(solution)/shard_map/all_gather | solution.py:43
  62.7 6.5 copy.31
  69.2 5.8 all-to-all-start
  75.2 4.7 multiply_convert_fusion.1
  79.9 31.4 %all-gather.9.cloned.1.call-done = bf16[384,8192]{1,0:T(8,128)(2,1)} async-done(((bf16[384,2048]{1,0:T(8,128)(2,1)}), bf16[384,8192]{1,0:T(8,128)(2,1)}) %all-gather.9.cloned.1.call-update) | async-done | bytes 6291472 | tf_op jit(solution)/shard_map/all_gather | solution.py:44
  111.3 6.5 copy.30
  117.8 95.9 %all-to-all-done = bf16[384,8,1024]{2,0,1:T(8,128)(2,1)} async-done(((bf16[384,8,1024]{2,0,1:T(8,128)(2,1)}), bf16[384,8,1024]{2,0,1:T(8,128)(2,1)}, u32[]{:S(2)}, u32[]{:S(2)}) %all-to-all-start) | async-done | bytes 6291488 | tf_op jit(solution)/shard_map/all_to_all | solution.py:51
  213.7 5.0 all-to-all-start.1
  220.1 6.5 copy.29
  226.6 129.8 %all-to-all-done.1 = bf16[384,8,1024]{2,0,1:T(8,128)(2,1)} async-done(((bf16[384,8,1024]{2,0,1:T(8,128)(2,1)}), bf16[384,8,1024]{2,0,1:T(8,128)(2,1)}, u32[]{:S(2)}, u32[]{:S(2)}) %all-to-all-start.1) | async-done | bytes 6291488 | tf_op jit(solution)/shard_map/all_to_all | solution.py:52
  356.4 4.8 all-to-all-start.2
  363.0 4.0 fusion.16
  367.1 8.9 %fusion.7 = f32[160,3072]{1,0:T(8,128)} fusion(bf16[1024,3072]{1,0:T(8,128)(2,1)} %all-gather.11.cloned.1.call-done, bf16[3072,1024]{1,0:T(8,128)(2,1)} %bitcast.3, f32[160,1024]{1,0:T(8,128)S(1)} %fusion.16, bf16[160,3072]{1,0:T(8,128)(2,1)S(1)} %copy-done, f32[160]{0:T(256)S(1)} %add_rsqrt_fusion.2, f32[160]{0:T(256)S(1)} %broadcast_multiply_fusion.4), kind=kOutput, calls=%fused_computation.25 | convolution fusion | flops 2016215040 | bytes 16188672 | tf_op jit(solution)/shard_map/dot_general | solution.py:18
  376.0 34.6 %all-gather.15.cloned.1.call-done = bf16[384,8192]{1,0:T(8,128)(2,1)} async-done(((bf16[384,2048]{1,0:T(8,128)(2,1)}), bf16[384,8192]{1,0:T(8,128)(2,1)}) %all-gather.15.cloned.1.call-update) | async-done | bytes 6291472 | tf_op jit(solution)/shard_map/all_gather | solution.py:46
  410.6 6.5 copy.28
  417.1 107.7 %all-to-all-done.2 = bf16[384,8,1024]{2,0,1:T(8,128)(2,1)} async-done(((bf16[384,8,1024]{2,0,1:T(8,128)(2,1)}), bf16[384,8,1024]{2,0,1:T(8,128)(2,1)}, u32[]{:S(2)}, u32[]{:S(2)}) %all-to-all-start.2) | async-done | bytes 6291488 | tf_op jit(solution)/shard_map/all_to_all | solution.py:53
  524.8 4.8 all-to-all-start.3
  529.7 3.3 convert_element_type.54
  533.2 138.3 %all-reduce.3.cloned.1.call-done = f32[160,3072]{1,0:T(8,128)} async-done(((f32[160,3072]{1,0:T(8,128)}), f32[160,3072]{1,0:T(8,128)}) %all-reduce.3.cloned.1.call-update) | async-done | bytes 1966096 | tf_op jit(solution)/shard_map/psum | solution.py:19
  671.5 2.3 fusion.10
  675.5 4.7 fusion.18
  680.1 36.9 %all-gather.17.cloned.1.call-done = bf16[1024,3072]{1,0:T(8,128)(2,1)} async-done(((bf16[1024,768]{1,0:T(8,128)(2,1)}), bf16[1024,3072]{1,0:T(8,128)(2,1)}) %all-gather.17.cloned.1.call-update) | async-done | bytes 6291472 | tf_op jit(solution)/shard_map/all_gather | solution.py:48
  717.1 8.2 fusion.6
  725.3 98.6 %all-reduce.5.cloned.1.call-done = f32[160,3072]{1,0:T(8,128)} async-done(((f32[160,3072]{1,0:T(8,128)}), f32[160,3072]{1,0:T(8,128)}) %all-reduce.5.cloned.1.call-update) | async-done | bytes 1966096 | tf_op jit(solution)/shard_map/psum | solution.py:19
  823.8 2.1 fusion.11
  828.0 6.4 copy.40
  834.4 6.3 copy.41
  840.7 2.7 copy.42
  843.4 6.4 copy.43
  849.8 6.3 copy.44
  856.2 2.7 copy.45
  (60 shorter events, 9.0 us)
Async XLA Ops:
  7.2 55.6 %all-gather.7.cloned.1.call-start = ((), (), s32[]{:S(2)}) async-start(), calls=%async_computation.4 | async-start | bytes 7864320 | tf_op jit(solution)/shard_map/all_gather | solution.py:43
  13.5 97.7 %all-gather.9.cloned.1.call-start = ((), (), s32[]{:S(2)}) async-start(), calls=%async_computation.5 | async-start | bytes 7864320 | tf_op jit(solution)/shard_map/all_gather | solution.py:44
  69.2 5.8 copy-start.6
  69.2 5.9 copy-start.3
  69.2 144.4 %all-to-all-start = ((bf16[384,8,1024]{2,0,1:T(8,128)(2,1)}), bf16[384,8,1024]{2,0,1:T(8,128)(2,1)}, u32[]{:S(2)}, u32[]{:S(2)}) async-start(bf16[384,8,1024]{2,0,1:T(8,128)(2,1)} %bitcast.38), calls=%async_computation | async-start | bytes 12582912 | tf_op jit(solution)/shard_map/all_to_all | solution.py:51
  75.0 145.1 %all-gather.13.cloned.1.call-start = ((), (), s32[]{:S(2)}) async-start(), calls=%async_computation.8 | async-start | bytes 7864320 | tf_op jit(solution)/shard_map/all_gather | solution.py:45
  213.7 5.1 copy-start.4
  213.7 142.7 %all-to-all-start.1 = ((bf16[384,8,1024]{2,0,1:T(8,128)(2,1)}), bf16[384,8,1024]{2,0,1:T(8,128)(2,1)}, u32[]{:S(2)}, u32[]{:S(2)}) async-start(bf16[384,8,1024]{2,0,1:T(8,128)(2,1)} %bitcast.39), calls=%async_computation.1 | async-start | bytes 12582912 | tf_op jit(solution)/shard_map/all_to_all | solution.py:52
  218.7 148.4 %all-gather.11.cloned.1.call-start = ((), (), s32[]{:S(2)}) async-start(), calls=%async_computation.6 | async-start | bytes 7864320 | tf_op jit(solution)/shard_map/all_gather | solution.py:47
  356.4 168.4 %all-to-all-start.2 = ((bf16[384,8,1024]{2,0,1:T(8,128)(2,1)}), bf16[384,8,1024]{2,0,1:T(8,128)(2,1)}, u32[]{:S(2)}, u32[]{:S(2)}) async-start(bf16[384,8,1024]{2,0,1:T(8,128)(2,1)} %bitcast.36), calls=%async_computation.2 | async-start | bytes 12582912 | tf_op jit(solution)/shard_map/all_to_all | solution.py:53
  361.2 1.2 copy-start
  361.2 49.4 %all-gather.15.cloned.1.call-start = ((), (), s32[]{:S(2)}) async-start(), calls=%async_computation.9 | async-start | bytes 7864320 | tf_op jit(solution)/shard_map/all_gather | solution.py:46
  361.8 309.7 %all-reduce.3.cloned.1.call-start = ((), (), s32[]{:S(2)}) async-start(), calls=%async_computation.7 | async-start | bytes 3932160 | tf_op jit(solution)/shard_map/psum | solution.py:19
  524.8 192.3 %all-to-all-start.3 = ((bf16[384,8,1024]{2,0,1:T(8,128)(2,1)}), bf16[384,8,1024]{2,0,1:T(8,128)(2,1)}, u32[]{:S(2)}, u32[]{:S(2)}) async-start(bf16[384,8,1024]{2,0,1:T(8,128)(2,1)} %bitcast.37), calls=%async_computation.3 | async-start | bytes 12582912 | tf_op jit(solution)/shard_map/all_to_all | solution.py:54
  529.6 3.6 copy-start.5
  529.6 187.4 %all-gather.17.cloned.1.call-start = ((), (), s32[]{:S(2)}) async-start(), calls=%async_computation.10 | async-start | bytes 7864320 | tf_op jit(solution)/shard_map/all_gather | solution.py:48
  533.0 290.8 %all-reduce.5.cloned.1.call-start = ((), (), s32[]{:S(2)}) async-start(), calls=%async_computation.11 | async-start | bytes 3932160 | tf_op jit(solution)/shard_map/psum | solution.py:19
  671.5 2.3 copy-start.1
  823.8 2.1 copy-start.2
  828.0 12.7 %slice-start = ((s8[6291456]{0:T(1024)(128)(4,1)}), s8[4194304]{0:T(1024)(128)(4,1)S(1)}, s32[]{:S(2)}) async-start(s8[6291456]{0:T(1024)(128)(4,1)} %bitcast.40), calls=%async_computation.12 | async-start | bytes 8388608
  834.4 6.4 slice-start.1
  843.4 12.7 %slice-start.2 = ((s8[6291456]{0:T(1024)(128)(4,1)}), s8[4194304]{0:T(1024)(128)(4,1)S(1)}, s32[]{:S(2)}) async-start(s8[6291456]{0:T(1024)(128)(4,1)} %bitcast.42), calls=%async_computation.14 | async-start | bytes 8388608
  849.8 6.4 slice-start.3
Sparse Core Ops, SparseCore 0:
  13.6 49.0 all-gather.6
  64.9 46.3 all-gather.8
  113.4 46.3 all-gather.12
  221.3 46.7 all-gather.10
  363.8 46.7 all-gather.14
  414.6 256.8 all-reduce.2
  673.6 43.3 all-gather.16
  725.4 98.3 all-reduce.4
where the time goes:
time: 866 us
  waiting for transfers between devices  723 us (83%)
  local copies, waits for them, and re-layouts  58.3 us (7%)
  matrix products  25.7 us (3%)
  other arithmetic  23.5 us (3%)
  starting transfers between devices  20.9 us (2%)
  between operations  14.3 us (2%)
    psum x2, waiting for transfers between devices, half_step(): block = lax.psum(partial_value, 'fs')  237 us
    all_to_all x1, waiting for transfers between devices, on_device(): lax.all_to_all(widened[1], 'fs', split_axis=1, concat_axis=0, tiled=True)  130 us
    all_to_all x1, waiting for transfers between devices, on_device(): lax.all_to_all(widened[2], 'fs', split_axis=1, concat_axis=0, tiled=True)  108 us
    all_to_all x1, waiting for transfers between devices, on_device(): lax.all_to_all(widened[0], 'fs', split_axis=1, concat_axis=0, tiled=True)  95.9 us
    all_gather x1, waiting for transfers between devices, on_device(): lax.all_gather(fold_gain(gate_first, gain_first), 'tp', axis=1, tiled=True)  48.5 us
    all_gather x1, waiting for transfers between devices, on_device(): lax.all_gather(down_second.astype(jnp.bfloat16), 'tp', axis=1, tiled=True)  36.9 us
    all_gather x1, waiting for transfers between devices, on_device(): lax.all_gather(fold_gain(up_second, gain_second), 'tp', axis=1, tiled=True)  34.6 us
    unnamed x28, local copies, waits for them, and re-layouts  31.5 us
  transfers between devices with their start and end apart: 12, of which 9 were waited for; matrix products, arithmetic and copies ran while one was open for 7% of the time, Pallas kernels for 0%

commit v1 on v0

--- a/solution.py
+++ b/solution.py
@@ -11,12 +11,32 @@
     return (values - center) * lax.rsqrt(spread + 1e-05)
 
 
+def sum_over_hidden(partial_value):
+    pieces = lax.all_to_all(
+        partial_value.astype(jnp.bfloat16), "fs", split_axis=1, concat_axis=0, tiled=True
+    )
+    rows = partial_value.shape[0]
+    pieces = pieces.reshape(-1, rows, pieces.shape[1]).astype(jnp.float32)
+    summed = jnp.sum(pieces, axis=0).astype(jnp.bfloat16)
+    return lax.all_gather(summed, "fs", axis=1, tiled=True).astype(jnp.float32)
+
+
+def regroup(folded):
+    spread = lax.all_to_all(folded, "tp", split_axis=0, concat_axis=1, tiled=True)
+    parts = lax.axis_size("fs")
+    rows = spread.shape[0]
+    owned = lax.all_to_all(spread, "fs", split_axis=1, concat_axis=0, tiled=True)
+    owned = owned.reshape(parts, rows, owned.shape[1])
+    whole = lax.all_gather(owned, "tp", axis=1, tiled=True)
+    return whole.reshape(-1, whole.shape[2])
+
+
 def half_step(normed, scales, w_gate, w_rising, w_down):
     gate_part = jnp.dot(normed, w_gate, preferred_element_type=jnp.float32)
     rising = jnp.dot(normed, w_rising, preferred_element_type=jnp.float32)
     hidden = (jax.nn.silu(gate_part) * rising).astype(jnp.bfloat16)
     partial_value = jnp.dot(hidden, w_down, preferred_element_type=jnp.float32)
-    block = lax.psum(partial_value, "fs")
+    block = sum_over_hidden(partial_value)
     mixed = 1.6817928 * scales[None, :] * normed.astype(jnp.float32) + 0.5 * block
     return plain_norm(mixed).astype(jnp.bfloat16)
 
@@ -39,23 +59,16 @@
         picked = lax.dynamic_slice_in_dim(scales, offset, row_count, 0)
         return (picked[:, None] * weight).astype(jnp.bfloat16)
 
-    widened = (
-        lax.all_gather(fold_gain(gate_first, gain_first), "tp", axis=1, tiled=True),
-        lax.all_gather(fold_gain(up_first, gain_first), "tp", axis=1, tiled=True),
-        lax.all_gather(fold_gain(gate_second, gain_second), "tp", axis=1, tiled=True),
-        lax.all_gather(fold_gain(up_second, gain_second), "tp", axis=1, tiled=True),
-        lax.all_gather(down_first.astype(jnp.bfloat16), "tp", axis=1, tiled=True),
-        lax.all_gather(down_second.astype(jnp.bfloat16), "tp", axis=1, tiled=True),
+    serve_gate_first = regroup(fold_gain(gate_first, gain_first))
+    serve_up_first = regroup(fold_gain(up_first, gain_first))
+    serve_down_first = lax.all_gather(
+        down_first.astype(jnp.bfloat16), "tp", axis=1, tiled=True
     )
-    regrouped = (
-        lax.all_to_all(widened[0], "fs", split_axis=1, concat_axis=0, tiled=True),
-        lax.all_to_all(widened[1], "fs", split_axis=1, concat_axis=0, tiled=True),
-        lax.all_to_all(widened[2], "fs", split_axis=1, concat_axis=0, tiled=True),
-        lax.all_to_all(widened[3], "fs", split_axis=1, concat_axis=0, tiled=True),
+    serve_gate_second = regroup(fold_gain(gate_second, gain_second))
+    serve_up_second = regroup(fold_gain(up_second, gain_second))
+    serve_down_second = lax.all_gather(
+        down_second.astype(jnp.bfloat16), "tp", axis=1, tiled=True
     )
-    serve_gate_first, serve_up_first, serve_gate_second, serve_up_second = regrouped
-    serve_down_first = widened[4]
-    serve_down_second = widened[5]
     normed_zero = plain_norm(tokens).astype(jnp.bfloat16)
     normed_one = half_step(
         normed_zero, gain_first, serve_gate_first, serve_up_first, serve_down_first

time: 866 us -> 531 us (0.61)
  waiting for transfers between devices: 723 us -> 29.1 us
  blocking collectives: 0 us -> 365 us
  local copies, waits for them, and re-layouts: 58.3 us -> 74 us
  starting transfers between devices: 20.9 us -> 7.57 us
  matrix products: 25.7 us -> 16.4 us
    all_to_all x4 -> x2, waiting for transfers between devices: 333 us -> 28.4 us  [sum_over_hidden(): lax.all_to_all(partial_value.astype(jnp.bfloat16), 'fs', split_axis=1, co...]
    all_to_all x0 -> x8, blocking collectives: none -> 298 us  [the longest x4 172 us: regroup(): lax.all_to_all(spread, 'fs', split_axis=1, concat_axis=0, tiled=True)]
    psum x2 -> x0, waiting for transfers between devices: 237 us -> none  [half_step(): block = lax.psum(partial_value, 'fs')]
    all_gather x4, waiting for transfers between devices: 114 us -> 0.5 us  [regroup(): whole = lax.all_gather(owned, 'tp', axis=1, tiled=True)]
    all_gather x0 -> x2, blocking collectives: none -> 67.3 us  [sum_over_hidden(): return lax.all_gather(summed, 'fs', axis=1, tiled=True).astype(jnp.float32)]
    all_gather x0 -> x4, local copies, waits for them, and re-layouts: none -> 36.9 us  [regroup(): whole = lax.all_gather(owned, 'tp', axis=1, tiled=True)]
    all_gather x1, waiting for transfers between devices: 36.9 us -> 0.02 us  [on_device(): lax.all_gather(down_second.astype(jnp.bfloat16), 'tp', axis=1, tiled=True)]
    unnamed x28 -> x20, local copies, waits for them, and re-layouts: 31.5 us -> 10.4 us
  transfers between devices with their start and end apart: 12 -> 8, of which waited for: 9 -> 3; matrix products, arithmetic and copies ran while one was open for 7% -> 14% of each run, Pallas kernels for 0% -> 0%
where the time goes in v1:
time: 531 us; the launch traced here: 523 us
  blocking collectives  365 us (69%)
  local copies, waits for them, and re-layouts  74 us (14%)
  waiting for transfers between devices  29.1 us (5%)
  matrix products  16.4 us (3%)
  other arithmetic  16.1 us (3%)
  between operations  14.8 us (3%)
  starting transfers between devices  7.57 us (1%)
    all_to_all x4, blocking collectives, regroup(): lax.all_to_all(spread, 'fs', split_axis=1, concat_axis=0, tiled=True)  172 us
    all_to_all x4, blocking collectives, regroup(): lax.all_to_all(folded, 'tp', split_axis=0, concat_axis=1, tiled=True)  126 us
    all_gather x2, blocking collectives, sum_over_hidden(): return lax.all_gather(summed, 'fs', axis=1, tiled=True).astype(jnp.float32)  67.3 us
    all_gather x4, local copies, waits for them, and re-layouts, regroup(): whole = lax.all_gather(owned, 'tp', axis=1, tiled=True)  36.9 us
    all_to_all x2, waiting for transfers between devices, sum_over_hidden(): lax.all_to_all(partial_value.astype(jnp.bfloat16), 'fs', split_axis=1, co...  28.4 us
    all_to_all x12, local copies, waits for them, and re-layouts, regroup(): lax.all_to_all(spread, 'fs', split_axis=1, concat_axis=0, tiled=True)  18.8 us
    dot_general x2, matrix products, half_step(): partial_value = jnp.dot(hidden, w_down, preferred_element_type=jnp.float32)  13.9 us
  transfers between devices with their start and end apart: 8, of which 3 were waited for; matrix products, arithmetic and copies ran while one was open for 14% of the time, Pallas kernels for 0%

profile of v1, /device:TPU:0, one launch (start us, length us, event | category | flops | bytes accessed | tf_op | source)
XLA Modules:
  0.0 523.0 jit_solution(2696292961990616382)
XLA Ops:
  8.0 3.7 multiply_convert_fusion.3
  11.7 24.1 %all_to_all.154 = bf16[4,96,2048]{2,1,0:T(8,128)(2,1)S(1)} all-to-all(bf16[4,96,2048]{2,1,0:T(8,128)(2,1)S(1)} %bitcast.44), channel_id=1, replica_groups=mesh['fs'=8,'tp'=4] {'tp'}, dimensions={0} | all-to-all | bytes 3145728 | tf_op jit(solution)/shard_map/all_to_all | solution.py:25
  37.0 1.8 all_to_all.119
  38.9 2.3 copy.29
  41.2 42.3 %all_to_all.155 = bf16[96,8,1024]{2,0,1:T(8,128)(2,1)S(1)} all-to-all(bf16[96,8,1024]{2,0,1:T(8,128)(2,1)S(1)} %copy.29), channel_id=1, replica_groups=mesh['fs'=8,'tp'=4] {'fs'}, dimensions={1} | all-to-all | bytes 3145728 | tf_op jit(solution)/shard_map/all_to_all | solution.py:28
  83.5 2.0 copy.30
  85.6 36.1 %all_to_all.156 = bf16[4,96,2048]{2,1,0:T(8,128)(2,1)S(1)} all-to-all(bf16[4,96,2048]{2,1,0:T(8,128)(2,1)S(1)} %bitcast.42), channel_id=1, replica_groups=mesh['fs'=8,'tp'=4] {'tp'}, dimensions={0} | all-to-all | bytes 3145728 | tf_op jit(solution)/shard_map/all_to_all | solution.py:25
  124.2 39.1 %all_to_all.157 = bf16[96,8,1024]{2,0,1:T(8,128)(2,1)S(1)} all-to-all(bf16[96,8,1024]{2,0,1:T(8,128)(2,1)S(1)} %copy.33), channel_id=1, replica_groups=mesh['fs'=8,'tp'=4] {'fs'}, dimensions={1} | all-to-all | bytes 3145728 | tf_op jit(solution)/shard_map/all_to_all | solution.py:28
  163.3 2.0 copy.34
  166.8 3.9 multiply_convert_fusion.1
  170.7 39.8 %all_to_all.158 = bf16[4,96,2048]{2,1,0:T(8,128)(2,1)S(1)} all-to-all(bf16[4,96,2048]{2,1,0:T(8,128)(2,1)S(1)} %bitcast.45), channel_id=1, replica_groups=mesh['fs'=8,'tp'=4] {'tp'}, dimensions={0} | all-to-all | bytes 3145728 | tf_op jit(solution)/shard_map/all_to_all | solution.py:25
  211.7 1.8 all_to_all.133
  213.6 2.3 copy.38
  215.8 51.1 %all_to_all.159 = bf16[96,8,1024]{2,0,1:T(8,128)(2,1)S(1)} all-to-all(bf16[96,8,1024]{2,0,1:T(8,128)(2,1)S(1)} %copy.38), channel_id=1, replica_groups=mesh['fs'=8,'tp'=4] {'fs'}, dimensions={1} | all-to-all | bytes 3145728 | tf_op jit(solution)/shard_map/all_to_all | solution.py:28
  266.9 2.0 copy.39
  269.0 26.1 %all_to_all.160 = bf16[4,96,2048]{2,1,0:T(8,128)(2,1)S(1)} all-to-all(bf16[4,96,2048]{2,1,0:T(8,128)(2,1)S(1)} %bitcast.43), channel_id=1, replica_groups=mesh['fs'=8,'tp'=4] {'tp'}, dimensions={0} | all-to-all | bytes 3145728 | tf_op jit(solution)/shard_map/all_to_all | solution.py:25
  297.6 39.2 %all_to_all.161 = bf16[96,8,1024]{2,0,1:T(8,128)(2,1)S(1)} all-to-all(bf16[96,8,1024]{2,0,1:T(8,128)(2,1)S(1)} %copy.42), channel_id=1, replica_groups=mesh['fs'=8,'tp'=4] {'fs'}, dimensions={1} | all-to-all | bytes 3145728 | tf_op jit(solution)/shard_map/all_to_all | solution.py:28
  336.8 2.0 copy.43
  342.0 9.7 %copy.31 = bf16[8,384,1024]{2,1,0:T(8,128)(2,1)} copy(bf16[8,384,1024]{2,0,1:T(8,128)(2,1)} %all-gather.7.cloned.1.call-done) | data formatting | bytes 12582912 | tf_op jit(solution)/shard_map/all_gather | solution.py:30
  351.7 9.2 %copy.35 = bf16[8,384,1024]{2,1,0:T(8,128)(2,1)} copy(bf16[8,384,1024]{2,0,1:T(8,128)(2,1)} %all-gather.9.cloned.1.call-done) | data formatting | bytes 12582912 | tf_op jit(solution)/shard_map/all_gather | solution.py:30
  362.3 7.0 %convolution_convert_fusion.1 = bf16[160,3072]{1,0:T(8,128)(2,1)S(1)} fusion(bf16[1024,3072]{1,0:T(8,128)(2,1)} %all-gather.11.cloned.1.call-done, bf16[3072,1024]{1,0:T(8,128)(2,1)} %bitcast.38, f32[160,1024]{1,0:T(8,128)S(1)} %fusion.14, bf16[160,3072]{1,0:T(8,128)(2,1)S(1)} %copy-done.1, f32[160]{0:T(256)S(1)} %add_rsqrt_fusion.2, ...), kind=kOutput, calls=%fused_computation.1 | convolution fusion | flops 2016706560 | bytes 15205632 | tf_op jit(solution)/shard_map/dot_general | solution.py:38
  370.3 3.8 all-to-all-start.4
  374.1 9.1 %copy.40 = bf16[8,384,1024]{2,1,0:T(8,128)(2,1)} copy(bf16[8,384,1024]{2,0,1:T(8,128)(2,1)} %all-gather.13.cloned.1.call-done) | data formatting | bytes 12582912 | tf_op jit(solution)/shard_map/all_gather | solution.py:30
  383.7 9.0 %copy.44 = bf16[8,384,1024]{2,1,0:T(8,128)(2,1)} copy(bf16[8,384,1024]{2,0,1:T(8,128)(2,1)} %all-gather.15.cloned.1.call-done) | data formatting | bytes 12582912 | tf_op jit(solution)/shard_map/all_gather | solution.py:30
  392.7 5.5 %all-to-all-done.4 = bf16[160,8,384]{2,0,1:T(8,128)(2,1)S(1)} async-done(((bf16[160,8,384]{2,0,1:T(8,128)(2,1)}), bf16[160,8,384]{2,0,1:T(8,128)(2,1)S(1)}, u32[]{:S(2)}, u32[]{:S(2)}) %all-to-all-start.4) | async-done | bytes 983072 | tf_op jit(solution)/shard_map/all_to_all | solution.py:15
  398.3 33.7 %all_gather.27 = bf16[160,3072]{1,0:T(8,128)(2,1)S(1)} all-gather(bf16[160,384]{1,0:T(8,128)(2,1)S(1)} %reduce_sum.80), channel_id=1, replica_groups=mesh['fs'=8,'tp'=4] {'fs'}, dimensions={1}, use_global_device_ids=true | all-gather | bytes 1105920 | tf_op jit(solution)/shard_map/all_gather | solution.py:21
  436.0 6.9 %convolution_convert_fusion = bf16[160,3072]{1,0:T(8,128)(2,1)S(1)} fusion(bf16[1024,3072]{1,0:T(8,128)(2,1)} %all-gather.17.cloned.1.call-done, bf16[160,3072]{1,0:T(8,128)(2,1)S(1)} %multiply_convert_fusion.5, bf16[3072,1024]{1,0:T(8,128)(2,1)} %bitcast.40, f32[160,1024]{1,0:T(8,128)S(1)} %fusion.16), kind=kOutput, calls=%fused_computation | convolution fusion | flops 2014740480 | bytes 15204352 | tf_op jit(solution)/shard_map/dot_general | solution.py:38
  444.0 3.6 all-to-all-start.9
  447.6 23.0 %all-to-all-done.9 = bf16[160,8,384]{2,0,1:T(8,128)(2,1)S(1)} async-done(((bf16[160,8,384]{2,0,1:T(8,128)(2,1)}), bf16[160,8,384]{2,0,1:T(8,128)(2,1)S(1)}, u32[]{:S(2)}, u32[]{:S(2)}) %all-to-all-start.9) | async-done | bytes 983072 | tf_op jit(solution)/shard_map/all_to_all | solution.py:15
  470.6 33.6 %all_gather.31 = bf16[160,3072]{1,0:T(8,128)(2,1)S(1)} all-gather(bf16[160,384]{1,0:T(8,128)(2,1)S(1)} %reduce_sum.83), channel_id=1, replica_groups=mesh['fs'=8,'tp'=4] {'fs'}, dimensions={1}, use_global_device_ids=true | all-gather | bytes 1105920 | tf_op jit(solution)/shard_map/all_gather | solution.py:21
  506.9 6.1 %copy.54 = bf16[1024,3072]{1,0:T(8,128)(2,1)} copy(bf16[1024,3072]{1,0:T(8,128)(2,1)} %all-gather.11.cloned.1.call-done) | data formatting | bytes 12582912
  513.0 2.7 copy.55
  (71 shorter events, 23.9 us)
Async XLA Ops:
  7.2 334.9 %all-gather.7.cloned.1.call-start = ((), (), s32[]{:S(2)}) async-start(), calls=%async_computation.10 | async-start | bytes 7864320 | tf_op jit(solution)/shard_map/all_gather | solution.py:30
  85.5 266.2 %all-gather.9.cloned.1.call-start = ((), (), s32[]{:S(2)}) async-start(), calls=%async_computation.11 | async-start | bytes 7864320 | tf_op jit(solution)/shard_map/all_gather | solution.py:30
  163.3 2.1 copy-start.3
  165.3 1.4 copy-start.6
  165.3 196.9 %all-gather.11.cloned.1.call-start = ((), (), s32[]{:S(2)}) async-start(), calls=%async_computation.12 | async-start | bytes 7864320 | tf_op jit(solution)/shard_map/all_gather | solution.py:64
  166.7 207.4 %all-gather.13.cloned.1.call-start = ((), (), s32[]{:S(2)}) async-start(), calls=%async_computation.13 | async-start | bytes 7864320 | tf_op jit(solution)/shard_map/all_gather | solution.py:30
  269.0 114.7 %all-gather.15.cloned.1.call-start = ((), (), s32[]{:S(2)}) async-start(), calls=%async_computation.14 | async-start | bytes 7864320 | tf_op jit(solution)/shard_map/all_gather | solution.py:30
  336.8 2.1 copy-start.4
  338.8 97.2 %all-gather.17.cloned.1.call-start = ((), (), s32[]{:S(2)}) async-start(), calls=%async_computation.15 | async-start | bytes 7864320 | tf_op jit(solution)/shard_map/all_gather | solution.py:69
  340.2 1.2 copy-start.1
  351.7 9.2 %copy-start.2 = (bf16[8,384,1024]{2,1,0:T(8,128)(2,1)S(1)}, bf16[8,384,1024]{2,1,0:T(8,128)(2,1)}, u32[]{:S(2)}) copy-start(bf16[8,384,1024]{2,1,0:T(8,128)(2,1)} %copy.31) | copy-start | bytes 18874372
  369.3 4.8 copy-start.5
  370.3 27.8 %all-to-all-start.4 = ((bf16[160,8,384]{2,0,1:T(8,128)(2,1)}), bf16[160,8,384]{2,0,1:T(8,128)(2,1)S(1)}, u32[]{:S(2)}, u32[]{:S(2)}) async-start(bf16[160,8,384]{2,0,1:T(8,128)(2,1)} %bitcast.31), calls=%async_computation.4 | async-start | bytes 1966080 | tf_op jit(solution)/shard_map/all_to_all | solution.py:15
  432.0 2.8 copy-start
  444.0 26.5 %all-to-all-start.9 = ((bf16[160,8,384]{2,0,1:T(8,128)(2,1)}), bf16[160,8,384]{2,0,1:T(8,128)(2,1)S(1)}, u32[]{:S(2)}, u32[]{:S(2)}) async-start(bf16[160,8,384]{2,0,1:T(8,128)(2,1)} %bitcast.30), calls=%async_computation.9 | async-start | bytes 1966080 | tf_op jit(solution)/shard_map/all_to_all | solution.py:15
  505.4 7.6 %slice-start = ((s8[6291456]{0:T(1024)(128)(4,1)}), s8[4194304]{0:T(1024)(128)(4,1)S(1)}, s32[]{:S(2)}) async-start(s8[6291456]{0:T(1024)(128)(4,1)} %bitcast.34), calls=%async_computation.16 | async-start | bytes 8388608
  506.9 6.1 %slice-start.1 = ((s8[6291456]{0:T(1024)(128)(4,1)}), s8[2097152]{0:T(1024)(128)(4,1)S(1)}, s32[]{:S(2)}) async-start(s8[6291456]{0:T(1024)(128)(4,1)} %bitcast.34), calls=%async_computation.17 | async-start | bytes 4194304
Sparse Core Ops, SparseCore 0:
  85.6 57.7 all-gather.6
  165.4 61.2 all-gather.8
  228.8 46.1 all-gather.10
  276.5 50.4 all-gather.12
  338.9 44.6 all-gather.14
  385.7 46.3 all-gather.16

commit v2 on v1

--- a/solution.py
+++ b/solution.py
@@ -1,7 +1,152 @@
 import jax
 import jax.numpy as jnp
 from jax import lax
+from jax.experimental import pallas as pl
+from jax.experimental.pallas import tpu as pltpu
 from jax.sharding import PartitionSpec as P
+
+import functools
+
+MESH = pl.DeviceIdType.MESH
+
+
+def can_push(parts, columns, rows, owned):
+    return parts == 4 and columns % owned == 0 and owned % 128 == 0 and rows % 128 == 0
+
+
+def move_kernel(parts, spans, rows, owned, a0, a1, o0, o1, *sems):
+    land_s, land_r, x_s, x_r, near_s, near_r, far_s, far_r = sems
+    fs = lax.axis_index("fs")
+    tp = lax.axis_index("tp")
+    plane = tp // 2
+    core = tp % 2
+    partner = plane * 2 + 1 - core
+    across = (1 - plane) * 2 + core
+    big = rows * 3 // 8
+    small = rows // 8
+    sources = (a0, a1)
+    results = (o0, o1)
+
+    def piece(is_big, of_core):
+        if is_big:
+            return of_core * big, big
+        return 2 * big + of_core * small, small
+
+    def window(m, origin, span):
+        start, length = span
+        return results[m].at[pl.ds(pl.multiple_of(origin * rows + start, 16), length), :]
+
+    def copy(src, dst, send, recv, to_fs, to_tp):
+        return pltpu.make_async_remote_copy(
+            src_ref=src,
+            dst_ref=dst,
+            send_sem=send,
+            recv_sem=recv,
+            device_id={"fs": to_fs, "tp": to_tp},
+            device_id_type=MESH,
+        )
+
+    sends = []
+    for m in range(2):
+        for k in range(spans):
+            shift = lax.rem(fs + k, spans)
+            to_fs = tp * spans + shift
+            columns = pl.ds(pl.multiple_of(shift * owned, 128), owned)
+            for turn in (1, 0):
+                for of_core in range(2):
+                    to_plane = plane if turn == 0 else 1 - plane
+                    to_tp = to_plane * 2 + of_core
+                    span = piece(turn == 0, of_core)
+                    src = sources[m].at[pl.ds(span[0], span[1]), columns]
+                    dst = window(m, fs, span)
+                    slot = turn * 2 + of_core
+                    sent = copy(src, dst, land_s.at[m, k, slot], land_r.at[m, fs], to_fs, to_tp)
+                    if turn == 1:
+                        sent.start()
+                        sends.append((sent, None))
+                    else:
+                        same = jnp.logical_and(to_fs == fs, to_tp == tp)
+                        pl.when(jnp.logical_not(same))(sent.start)
+                        kept = pltpu.make_async_copy(src, dst, land_r.at[m, fs])
+                        pl.when(same)(kept.start)
+                        sends.append((sent, same))
+
+    def receive(lands_big):
+        mine = piece(lands_big, core)
+        theirs = piece(not lands_big, core)
+        near = piece(lands_big, 1 - core)
+        far = piece(not lands_big, 1 - core)
+
+        def to_partner(m, s, span, send, recv):
+            part = window(m, s, span)
+            return copy(part, part, send.at[m, s], recv.at[m, s], fs, partner)
+
+        def to_across(m, s, span):
+            part = window(m, s, span)
+            return copy(part, part, x_s.at[m, s], x_r.at[m, s], fs, across)
+
+        for m in range(2):
+
+            @pl.loop(0, parts)
+            def _(j, m=m):
+                s = lax.rem(fs + j, parts)
+                part = window(m, s, mine)
+                copy(part, part, x_s.at[m, s], land_r.at[m, s], fs, across).wait_recv()
+                to_across(m, s, mine).start()
+                to_partner(m, s, mine, near_s, near_r).start()
+
+        for m in range(2):
+
+            @pl.loop(0, parts)
+            def _(j, m=m):
+                s = lax.rem(fs + j, parts)
+                to_across(m, s, theirs).wait_recv()
+                to_partner(m, s, theirs, far_s, far_r).start()
+
+        for m in range(2):
+
+            @pl.loop(0, parts)
+            def _(j, m=m):
+                s = lax.rem(fs + j, parts)
+                to_partner(m, s, near, near_s, near_r).wait_recv()
+                to_partner(m, s, far, far_s, far_r).wait_recv()
+                to_across(m, s, mine).wait_send()
+                to_partner(m, s, mine, near_s, near_r).wait_send()
+                to_partner(m, s, theirs, far_s, far_r).wait_send()
+
+    own = (fs // spans) // 2 == plane
+    pl.when(own)(functools.partial(receive, True))
+    pl.when(jnp.logical_not(own))(functools.partial(receive, False))
+
+    for sent, same in sends:
+        if same is None:
+            sent.wait_send()
+        else:
+            pl.when(jnp.logical_not(same))(sent.wait_send)
+
+
+def move(first, second):
+    parts = lax.axis_size("fs")
+    rows, columns = first.shape
+    owned = columns * lax.axis_size("tp") // parts
+    spans = columns // owned if columns % owned == 0 else 0
+    if not can_push(lax.axis_size("tp"), columns, rows, owned):
+        return regroup(first), regroup(second)
+    shape = jax.ShapeDtypeStruct((rows * parts, owned), first.dtype)
+    per_source = pltpu.SemaphoreType.DMA((2, parts))
+    moved = 2 * rows * parts * owned * 2
+    return pl.pallas_call(
+        functools.partial(move_kernel, parts, spans, rows, owned),
+        out_shape=(shape, shape),
+        in_specs=[pl.BlockSpec(memory_space=pl.ANY)] * 2,
+        out_specs=(pl.BlockSpec(memory_space=pl.ANY),) * 2,
+        scratch_shapes=[pltpu.SemaphoreType.DMA((2, spans, 4))] + [per_source] * 7,
+        compiler_params=pltpu.CompilerParams(has_side_effects=True),
+        cost_estimate=pl.CostEstimate(
+            flops=0, bytes_accessed=16 * moved, transcendentals=0
+        ),
+        name="move_blocks",
+    )(first, second)
 
 
 def plain_norm(values):
@@ -31,12 +176,14 @@
     return whole.reshape(-1, whole.shape[2])
 
 
-def half_step(normed, scales, w_gate, w_rising, w_down):
+def hidden_part(normed, w_gate, w_rising, w_down):
     gate_part = jnp.dot(normed, w_gate, preferred_element_type=jnp.float32)
     rising = jnp.dot(normed, w_rising, preferred_element_type=jnp.float32)
     hidden = (jax.nn.silu(gate_part) * rising).astype(jnp.bfloat16)
-    partial_value = jnp.dot(hidden, w_down, preferred_element_type=jnp.float32)
-    block = sum_over_hidden(partial_value)
+    return jnp.dot(hidden, w_down, preferred_element_type=jnp.float32)
+
+
+def finish(normed, scales, block):
     mixed = 1.6817928 * scales[None, :] * normed.astype(jnp.float32) + 0.5 * block
     return plain_norm(mixed).astype(jnp.bfloat16)
 
@@ -59,23 +206,29 @@
         picked = lax.dynamic_slice_in_dim(scales, offset, row_count, 0)
         return (picked[:, None] * weight).astype(jnp.bfloat16)
 
-    serve_gate_first = regroup(fold_gain(gate_first, gain_first))
-    serve_up_first = regroup(fold_gain(up_first, gain_first))
+    serve_gate_first, serve_up_first = move(
+        fold_gain(gate_first, gain_first), fold_gain(up_first, gain_first)
+    )
     serve_down_first = lax.all_gather(
         down_first.astype(jnp.bfloat16), "tp", axis=1, tiled=True
     )
-    serve_gate_second = regroup(fold_gain(gate_second, gain_second))
-    serve_up_second = regroup(fold_gain(up_second, gain_second))
+    normed_zero = plain_norm(tokens).astype(jnp.bfloat16)
+    partial_first = hidden_part(
+        normed_zero, serve_gate_first, serve_up_first, serve_down_first
+    )
+    partial_first, gate_folded, up_folded = lax.optimization_barrier(
+        (partial_first, fold_gain(gate_second, gain_second), fold_gain(up_second, gain_second))
+    )
+    serve_gate_second, serve_up_second = move(gate_folded, up_folded)
     serve_down_second = lax.all_gather(
         down_second.astype(jnp.bfloat16), "tp", axis=1, tiled=True
     )
-    normed_zero = plain_norm(tokens).astype(jnp.bfloat16)
-    normed_one = half_step(
-        normed_zero, gain_first, serve_gate_first, serve_up_first, serve_down_first
-    )
-    result_rows = half_step(
-        normed_one, gain_second, serve_gate_second, serve_up_second, serve_down_second
-    )
+    block_first = lax.psum(partial_first, "fs")
+    normed_one = finish(normed_zero, gain_first, block_first)
+    partial_second = hidden_part(
+        normed_one, serve_gate_second, serve_up_second, serve_down_second
+    )
+    result_rows = finish(normed_one, gain_second, sum_over_hidden(partial_second))
     return (
         result_rows,
         serve_gate_first,

time: 531 us -> 621 us (1.17)
  Pallas kernels: 0 us -> 421 us
  blocking collectives: 365 us -> 32.9 us
  local copies, waits for them, and re-layouts: 74 us -> 29.2 us
  starting transfers between devices: 7.57 us -> 27.2 us
  waiting for transfers between devices: 29.1 us -> 44.8 us
    pallas_call x0 -> x2, Pallas kernels: none -> 421 us  [move(): pl.pallas_call(functools.partial(move_kernel, parts, spans, rows, owned),...]
    all_to_all x8 -> x0, blocking collectives: 298 us -> none  [the longest x4 172 us: regroup(): lax.all_to_all(spread, 'fs', split_axis=1, concat_axis=0, tiled=True)]
    all_gather x4 -> x0, local copies, waits for them, and re-layouts: 36.9 us -> none  [regroup(): whole = lax.all_gather(owned, 'tp', axis=1, tiled=True)]
    all_gather x2 -> x1, blocking collectives: 67.3 us -> 32.9 us  [sum_over_hidden(): return lax.all_gather(summed, 'fs', axis=1, tiled=True).astype(jnp.float32)]
    all_to_all x16 -> x0, local copies, waits for them, and re-layouts: 23.7 us -> none  [the longest x12 18.8 us: regroup(): lax.all_to_all(spread, 'fs', split_axis=1, concat_axis=0, tiled=True)]
    all_gather x1, waiting for transfers between devices: 0.02 us -> 22.3 us  [on_device(): lax.all_gather(down_second.astype(jnp.bfloat16), 'tp', axis=1, tiled=True)]
    all_to_all x2 -> x1, starting transfers between devices: 7.32 us -> 27 us  [sum_over_hidden(): lax.all_to_all(partial_value.astype(jnp.bfloat16), 'fs', split_axis=1, co...]
    unnamed x20 -> x42, local copies, waits for them, and re-layouts: 10.4 us -> 28 us
  transfers between devices with their start and end apart: 8 -> 4, of which waited for: 3 -> 2; matrix products, arithmetic and copies ran while one was open for 14% -> 3% of each run, Pallas kernels for 0% -> 69%
where the time goes in v2:
time: 621 us; the launch traced here: 610 us
  Pallas kernels  421 us (68%)
  waiting for transfers between devices  44.8 us (7%)
  blocking collectives  32.9 us (5%)
  local copies, waits for them, and re-layouts  29.2 us (5%)
  starting transfers between devices  27.2 us (4%)
  other arithmetic  21 us (3%)
  matrix products  20.5 us (3%)
  between operations  14 us (2%)
    pallas_call x2, Pallas kernels, move(): pl.pallas_call(functools.partial(move_kernel, parts, spans, rows, owned),...  421 us
    all_gather x1, blocking collectives, sum_over_hidden(): return lax.all_gather(summed, 'fs', axis=1, tiled=True).astype(jnp.float32)  32.9 us
    unnamed x42, local copies, waits for them, and re-layouts  28 us
    all_to_all x1, starting transfers between devices, sum_over_hidden(): lax.all_to_all(partial_value.astype(jnp.bfloat16), 'fs', split_axis=1, co...  27 us
    all_to_all x1, waiting for transfers between devices, sum_over_hidden(): lax.all_to_all(partial_value.astype(jnp.bfloat16), 'fs', split_axis=1, co...  22.4 us
    all_gather x1, waiting for transfers between devices, on_device(): lax.all_gather(down_second.astype(jnp.bfloat16), 'tp', axis=1, tiled=True)  22.3 us
    dot_general x2, matrix products, hidden_part(): return jnp.dot(hidden, w_down, preferred_element_type=jnp.float32)  15.1 us
  transfers between devices with their start and end apart: 4, of which 2 were waited for; matrix products, arithmetic and copies ran while one was open for 3% of the time, Pallas kernels for 69%

profile of v2, /device:TPU:0, one launch (start us, length us, event | category | flops | bytes accessed | tf_op | source)
XLA Modules:
  0.0 610.0 jit_solution(12466194297071751309)
XLA Ops:
  7.2 3.3 convert_element_type.56
  10.8 4.5 multiply_convert_fusion.2
  15.3 179.9 %move_blocks.2 = (bf16[3072,1024]{1,0:T(8,128)(2,1)}, bf16[3072,1024]{1,0:T(8,128)(2,1)}) custom-call(bf16[384,2048]{1,0:T(8,128)(2,1)} %get-tuple-element.24.a0, bf16[384,2048]{1,0:T(8,128)(2,1)} %get-tuple-element.23.a1), custom_call_target="tpu_custom_call" | custom-call | bytes 201326592 | tf_op jit(solution)/shard_map/move_blocks/pallas_call | solution.py:138
  195.9 4.2 fusion.15
  200.6 2.7 multiply_convert_fusion
  203.2 8.2 %fusion.7 = f32[160,3072]{1,0:T(8,128)} fusion(bf16[1024,3072]{1,0:T(8,128)(2,1)} %all-gather.3.cloned.1.call-done, bf16[3072,1024]{1,0:T(8,128)(2,1)} %get-tuple-element.34, f32[160,1024]{1,0:T(8,128)S(1)} %fusion.15, bf16[160,3072]{1,0:T(8,128)(2,1)S(1)} %copy-done.1, f32[160]{0:T(256)S(1)} %add_rsqrt_fusion.2, f32[160]{0:T(256)S(1)} %broadcast_multiply_fusion.4), kind=kOutput, calls=%fused_computation.23 | convolution fusion | flops 2016215040 | bytes 16188672 | tf_op jit(solution)/shard_map/dot_general | solution.py:183
  211.5 3.2 convert_element_type.62
  214.8 240.6 %move_blocks.3 = (bf16[3072,1024]{1,0:T(8,128)(2,1)}, bf16[3072,1024]{1,0:T(8,128)(2,1)}) custom-call(bf16[384,2048]{1,0:T(8,128)(2,1)} %get-tuple-element.17.a0, bf16[384,2048]{1,0:T(8,128)(2,1)} %get-tuple-element.18.a1), custom_call_target="tpu_custom_call" | custom-call | bytes 201326592 | tf_op jit(solution)/shard_map/move_blocks/pallas_call | solution.py:138
  455.4 2.3 fusion.10
  457.8 0.8 multiply_reduce_fusion.1
  458.6 0.9 multiply_convert_fusion.5
  459.5 1.1 copy-done
  460.6 1.3 fusion.17
  461.8 22.3 %all-gather.5.cloned.1.call-done = bf16[1024,3072]{1,0:T(8,128)(2,1)} async-done(((bf16[1024,768]{1,0:T(8,128)(2,1)}), bf16[1024,3072]{1,0:T(8,128)(2,1)}) %all-gather.5.cloned.1.call-update) | async-done | bytes 6291472 | tf_op jit(solution)/shard_map/all_gather | solution.py:223
  484.1 6.9 %convolution_convert_fusion = bf16[160,3072]{1,0:T(8,128)(2,1)S(1)} fusion(bf16[1024,3072]{1,0:T(8,128)(2,1)} %all-gather.5.cloned.1.call-done, bf16[160,3072]{1,0:T(8,128)(2,1)S(1)} %multiply_convert_fusion.5, bf16[3072,1024]{1,0:T(8,128)(2,1)} %get-tuple-element.37, f32[160,1024]{1,0:T(8,128)S(1)} %fusion.17), kind=kOutput, calls=%fused_computation | convolution fusion | flops 2014740480 | bytes 15204352 | tf_op jit(solution)/shard_map/dot_general | solution.py:183
  491.0 1.0 copy.19
  492.0 27.0 %all-to-all-start = ((bf16[160,8,384]{2,0,1:T(8,128)(2,1)}), bf16[160,8,384]{2,0,1:T(8,128)(2,1)S(1)}, u32[]{:S(2)}, u32[]{:S(2)}) async-start(bf16[160,8,384]{2,0,1:T(8,128)(2,1)} %bitcast.11), calls=%async_computation | async-start | bytes 1966080 | tf_op jit(solution)/shard_map/all_to_all | solution.py:160
  519.1 22.4 %all-to-all-done = bf16[160,8,384]{2,0,1:T(8,128)(2,1)S(1)} async-done(((bf16[160,8,384]{2,0,1:T(8,128)(2,1)}), bf16[160,8,384]{2,0,1:T(8,128)(2,1)S(1)}, u32[]{:S(2)}, u32[]{:S(2)}) %all-to-all-start) | async-done | bytes 983072 | tf_op jit(solution)/shard_map/all_to_all | solution.py:160
  541.7 32.9 %all_gather.11 = bf16[160,3072]{1,0:T(8,128)(2,1)S(1)} all-gather(bf16[160,384]{1,0:T(8,128)(2,1)S(1)} %reduce_sum.70), channel_id=1, replica_groups=mesh['fs'=8,'tp'=4] {'fs'}, dimensions={1}, use_global_device_ids=true | all-gather | bytes 1105920 | tf_op jit(solution)/shard_map/all_gather | solution.py:166
  574.5 0.5 fusion.4
  575.0 0.6 multiply_reduce_fusion
  575.6 1.5 multiply_convert_fusion.4
  577.1 6.4 %copy.27 = bf16[3072,1024]{1,0:T(8,128)(2,1)} copy(bf16[3072,1024]{1,0:T(8,128)(2,1)} %get-tuple-element.33) | data formatting | bytes 12582912
  583.5 3.2 copy.28
  586.8 3.2 copy.29
  590.0 0.8 slice-done
  590.8 0.8 slice-done.1
  591.6 3.2 copy.30
  594.8 1.4 slice-done.9
  596.2 3.2 copy.31
  599.4 1.4 slice-done.7
  600.8 2.7 copy.32
  (57 shorter events, 1.7 us)
Async XLA Ops:
  7.2 3.5 copy-start.6
  7.2 3.6 copy-start.7
  7.2 196.0 %all-gather.3.cloned.1.call-start = ((), (), s32[]{:S(2)}) async-start(), calls=%async_computation.1 | async-start | bytes 7864320 | tf_op jit(solution)/shard_map/all_gather | solution.py:212
  7.2 3.6 copy-start.3
  10.6 444.8 %all-reduce.2.cloned.1.call-start = ((), (), s32[]{:S(2)}) async-start(), calls=%async_computation.2 | async-start | bytes 3932160 | tf_op jit(solution)/shard_map/psum | solution.py:226
  15.3 179.9 %copy-start.1 = (bf16[160,3072]{1,0:T(8,128)(2,1)S(1)}, bf16[160,3072]{1,0:T(8,128)(2,1)}, u32[]{:S(2)}) copy-start(bf16[160,3072]{1,0:T(8,128)(2,1)} %param.9) | copy-start | bytes 2949124
  195.9 4.2 copy-start.4
  195.9 4.7 copy-start.5
  211.5 272.6 %all-gather.5.cloned.1.call-start = ((), (), s32[]{:S(2)}) async-start(), calls=%async_computation.3 | async-start | bytes 7864320 | tf_op jit(solution)/shard_map/all_gather | solution.py:223
  455.4 2.4 copy-start.2
  457.8 2.8 copy-start
  492.0 49.5 %all-to-all-start = ((bf16[160,8,384]{2,0,1:T(8,128)(2,1)}), bf16[160,8,384]{2,0,1:T(8,128)(2,1)S(1)}, u32[]{:S(2)}, u32[]{:S(2)}) async-start(bf16[160,8,384]{2,0,1:T(8,128)(2,1)} %bitcast.11), calls=%async_computation | async-start | bytes 1966080 | tf_op jit(solution)/shard_map/all_to_all | solution.py:160
  575.6 7.9 %slice-start.4 = ((s8[6291456]{0:T(1024)(128)(4,1)}), s8[4194304]{0:T(1024)(128)(4,1)S(1)}, s32[]{:S(2)}) async-start(s8[6291456]{0:T(1024)(128)(4,1)} %bitcast.16), calls=%async_computation.8 | async-start | bytes 8388608
  577.1 6.4 %slice-start.5 = ((s8[6291456]{0:T(1024)(128)(4,1)}), s8[2097152]{0:T(1024)(128)(4,1)S(1)}, s32[]{:S(2)}) async-start(s8[6291456]{0:T(1024)(128)(4,1)} %bitcast.16), calls=%async_computation.9 | async-start | bytes 4194304
  577.1 9.6 %slice-start.2 = ((s8[6291456]{0:T(1024)(128)(4,1)}), s8[4194304]{0:T(1024)(128)(4,1)S(1)}, s32[]{:S(2)}) async-start(s8[6291456]{0:T(1024)(128)(4,1)} %bitcast.14), calls=%async_computation.6 | async-start | bytes 8388608
  583.5 3.2 slice-start.3
  583.5 7.2 %slice-start = ((s8[6291456]{0:T(1024)(128)(4,1)}), s8[4194304]{0:T(1024)(128)(4,1)S(1)}, s32[]{:S(2)}) async-start(s8[6291456]{0:T(1024)(128)(4,1)} %bitcast.12), calls=%async_computation.4 | async-start | bytes 8388608
  586.8 4.8 slice-start.1
  586.8 8.0 %slice-start.8 = ((s8[6291456]{0:T(1024)(128)(4,1)}), s8[2097152]{0:T(1024)(128)(4,1)S(1)}, s32[]{:S(2)}) async-start(s8[6291456]{0:T(1024)(128)(4,1)} %bitcast.20), calls=%async_computation.12 | async-start | bytes 4194304
  591.6 4.6 slice-start.9
  591.6 7.8 %slice-start.6 = ((s8[6291456]{0:T(1024)(128)(4,1)}), s8[2097152]{0:T(1024)(128)(4,1)S(1)}, s32[]{:S(2)}) async-start(s8[6291456]{0:T(1024)(128)(4,1)} %bitcast.18), calls=%async_computation.10 | async-start | bytes 4194304
  596.2 4.6 slice-start.7
Sparse Core Ops, SparseCore 0:
  10.7 93.1 all-gather.2
  211.6 214.7 all-reduce.1
  428.5 55.5 all-gather.4

commit v3 on v1

--- a/solution.py
+++ b/solution.py
@@ -1,7 +1,106 @@
 import jax
 import jax.numpy as jnp
 from jax import lax
+from jax.experimental import pallas as pl
+from jax.experimental.pallas import tpu as pltpu
 from jax.sharding import PartitionSpec as P
+
+import functools
+
+MESH = pl.DeviceIdType.MESH
+
+
+def can_push(members, parts, columns, rows):
+    blocks = parts // members
+    if parts % members or columns % (blocks * 128):
+        return False
+    return rows % (members * 16) == 0
+
+
+def scatter_kernel(parts, members, source, result, send_sems, recv_sems):
+    fs = lax.axis_index("fs")
+    tp = lax.axis_index("tp")
+    blocks = parts // members
+    rows = source.shape[0] // members
+    owned = source.shape[1] // blocks
+    landing = result.at[pl.ds(pl.multiple_of(fs * rows, 16), rows), :]
+
+    sends = []
+    for k in range(blocks):
+        block = lax.rem(fs + k, blocks)
+        to_fs = tp * blocks + block
+        columns = pl.ds(pl.multiple_of(block * owned, 128), owned)
+        for q in range(members):
+            to_tp = lax.rem(tp + q, members)
+            src = source.at[pl.ds(pl.multiple_of(to_tp * rows, 16), rows), columns]
+            sent = pltpu.make_async_remote_copy(
+                src_ref=src,
+                dst_ref=landing,
+                send_sem=send_sems.at[k, q],
+                recv_sem=recv_sems.at[fs],
+                device_id={"fs": to_fs, "tp": to_tp},
+                device_id_type=MESH,
+            )
+            if q:
+                sent.start()
+                sends.append((sent, None))
+                continue
+            same = to_fs == fs
+            pl.when(jnp.logical_not(same))(sent.start)
+            pl.when(same)(pltpu.make_async_copy(src, landing, recv_sems.at[fs]).start)
+            sends.append((sent, same))
+
+    for s in range(parts):
+        part = result.at[pl.ds(s * rows, rows), :]
+        pltpu.make_async_remote_copy(
+            src_ref=part,
+            dst_ref=part,
+            send_sem=send_sems.at[0, 0],
+            recv_sem=recv_sems.at[s],
+            device_id={"fs": fs, "tp": lax.rem(tp + 1, members)},
+            device_id_type=MESH,
+        ).wait_recv()
+
+    for sent, same in sends:
+        if same is None:
+            sent.wait_send()
+        else:
+            pl.when(jnp.logical_not(same))(sent.wait_send)
+
+
+def scatter(folded):
+    parts = lax.axis_size("fs")
+    members = lax.axis_size("tp")
+    rows, columns = folded.shape
+    blocks = parts // members
+    shape = (parts * rows // members, columns // blocks)
+    moved = 2 * shape[0] * shape[1]
+    return pl.pallas_call(
+        functools.partial(scatter_kernel, parts, members),
+        out_shape=jax.ShapeDtypeStruct(shape, folded.dtype),
+        in_specs=[pl.BlockSpec(memory_space=pl.ANY)],
+        out_specs=pl.BlockSpec(memory_space=pl.ANY),
+        scratch_shapes=[
+            pltpu.SemaphoreType.DMA((blocks, members)),
+            pltpu.SemaphoreType.DMA((parts,)),
+        ],
+        compiler_params=pltpu.CompilerParams(has_side_effects=True),
+        cost_estimate=pl.CostEstimate(
+            flops=0, bytes_accessed=64 * moved, transcendentals=0
+        ),
+        name="scatter_pieces",
+    )(folded)
+
+
+def widen(pieces):
+    return ordered(lax.all_gather(pieces, "tp", axis=0))
+
+
+def ordered(gathered):
+    parts = lax.axis_size("fs")
+    members, rows, owned = gathered.shape
+    split = gathered.reshape(members, parts, rows // parts, owned)
+    return split.transpose(1, 0, 2, 3).reshape(members * rows, owned)
 
 
 def plain_norm(values):
@@ -31,12 +130,14 @@
     return whole.reshape(-1, whole.shape[2])
 
 
-def half_step(normed, scales, w_gate, w_rising, w_down):
+def hidden_part(normed, w_gate, w_rising, w_down):
     gate_part = jnp.dot(normed, w_gate, preferred_element_type=jnp.float32)
     rising = jnp.dot(normed, w_rising, preferred_element_type=jnp.float32)
     hidden = (jax.nn.silu(gate_part) * rising).astype(jnp.bfloat16)
-    partial_value = jnp.dot(hidden, w_down, preferred_element_type=jnp.float32)
-    block = sum_over_hidden(partial_value)
+    return jnp.dot(hidden, w_down, preferred_element_type=jnp.float32)
+
+
+def finish(normed, scales, block):
     mixed = 1.6817928 * scales[None, :] * normed.astype(jnp.float32) + 0.5 * block
     return plain_norm(mixed).astype(jnp.bfloat16)
 
@@ -59,23 +160,46 @@
         picked = lax.dynamic_slice_in_dim(scales, offset, row_count, 0)
         return (picked[:, None] * weight).astype(jnp.bfloat16)
 
-    serve_gate_first = regroup(fold_gain(gate_first, gain_first))
-    serve_up_first = regroup(fold_gain(up_first, gain_first))
-    serve_down_first = lax.all_gather(
-        down_first.astype(jnp.bfloat16), "tp", axis=1, tiled=True
-    )
-    serve_gate_second = regroup(fold_gain(gate_second, gain_second))
-    serve_up_second = regroup(fold_gain(up_second, gain_second))
+    folded = (
+        fold_gain(gate_first, gain_first),
+        fold_gain(up_first, gain_first),
+        fold_gain(gate_second, gain_second),
+        fold_gain(up_second, gain_second),
+    )
+    down_rounded, scattered_first = lax.optimization_barrier(
+        (down_first.astype(jnp.bfloat16), folded[0])
+    )
+    folded = (scattered_first,) + folded[1:]
+    serve_down_first = lax.all_gather(down_rounded, "tp", axis=1, tiled=True)
     serve_down_second = lax.all_gather(
         down_second.astype(jnp.bfloat16), "tp", axis=1, tiled=True
     )
     normed_zero = plain_norm(tokens).astype(jnp.bfloat16)
-    normed_one = half_step(
-        normed_zero, gain_first, serve_gate_first, serve_up_first, serve_down_first
-    )
-    result_rows = half_step(
-        normed_one, gain_second, serve_gate_second, serve_up_second, serve_down_second
-    )
+    members = lax.axis_size("tp")
+    if can_push(members, lax.axis_size("fs"), gate_first.shape[1], row_count):
+        pieces = [scatter(folded[0])]
+        for weight in folded[1:]:
+            weight, pieces[-1] = lax.optimization_barrier((weight, pieces[-1]))
+            pieces.append(scatter(weight))
+        normed_zero, pieces[3] = lax.optimization_barrier((normed_zero, pieces[3]))
+        served = [widen(piece) for piece in pieces[:2]]
+        later = [lax.all_gather(piece, "tp", axis=0) for piece in pieces[2:]]
+    else:
+        served = [regroup(weight) for weight in folded]
+        later = []
+    serve_gate_first, serve_up_first = served[:2]
+    partial_first = hidden_part(
+        normed_zero, serve_gate_first, serve_up_first, serve_down_first
+    )
+    normed_one = finish(normed_zero, gain_first, sum_over_hidden(partial_first))
+    if later:
+        normed_one, *later = lax.optimization_barrier((normed_one, *later))
+        served += [ordered(gathered) for gathered in later]
+    serve_gate_second, serve_up_second = served[2:]
+    partial_second = hidden_part(
+        normed_one, serve_gate_second, serve_up_second, serve_down_second
+    )
+    result_rows = finish(normed_one, gain_second, sum_over_hidden(partial_second))
     return (
         result_rows,
         serve_gate_first,

time: 531 us -> 559 us (1.053); the launches traced: 523 us -> 558 us
  blocking collectives: 365 us -> 66.5 us
  Pallas kernels: 0 us -> 293 us
  waiting for transfers between devices: 29.1 us -> 94.4 us
  local copies, waits for them, and re-layouts: 74 us -> 33 us
  starting transfers between devices: 7.57 us -> 18.9 us
    all_to_all x8 -> x0, blocking collectives: 298 us -> none  [the longest x4 172 us: regroup(): lax.all_to_all(spread, 'fs', split_axis=1, concat_axis=0, tiled=True)]
    pallas_call x0 -> x4, Pallas kernels: none -> 293 us  [scatter(): pl.pallas_call(functools.partial(scatter_kernel, parts, members), out_sha...]
    all_gather x1, waiting for transfers between devices: 0.02 us -> 38.6 us  [on_device(): lax.all_gather(down_second.astype(jnp.bfloat16), 'tp', axis=1, tiled=True)]
    all_gather x4 -> x0, local copies, waits for them, and re-layouts: 36.9 us -> none  [regroup(): whole = lax.all_gather(owned, 'tp', axis=1, tiled=True)]
    all_to_all x16 -> x0, local copies, waits for them, and re-layouts: 23.7 us -> none  [the longest x12 18.8 us: regroup(): lax.all_to_all(spread, 'fs', split_axis=1, concat_axis=0, tiled=True)]
    all_to_all x2, waiting for transfers between devices: 28.4 us -> 50.9 us  [sum_over_hidden(): lax.all_to_all(partial_value.astype(jnp.bfloat16), 'fs', split_axis=1, co...]
    transpose x0 -> x2, local copies, waits for them, and re-layouts: none -> 13.4 us  [ordered(): return split.transpose(1, 0, 2, 3).reshape(members * rows, owned)]
    all_to_all x2, starting transfers between devices: 7.32 us -> 18.6 us  [sum_over_hidden(): lax.all_to_all(partial_value.astype(jnp.bfloat16), 'fs', split_axis=1, co...]
  transfers between devices with their start and end apart: 8 -> 8, of which waited for: 3 -> 4; matrix products, arithmetic and copies ran while one was open for 14% -> 8% of each run, Pallas kernels for 0% -> 40%
where the time goes in v3:
time: 559 us; the launch traced here: 558 us
  Pallas kernels  293 us (52%)
  waiting for transfers between devices  94.4 us (17%)
  blocking collectives  66.5 us (12%)
  local copies, waits for them, and re-layouts  33 us (6%)
  other arithmetic  21 us (4%)
  starting transfers between devices  18.9 us (3%)
  matrix products  17.9 us (3%)
  between operations  14.3 us (3%)
    pallas_call x4, Pallas kernels, scatter(): pl.pallas_call(functools.partial(scatter_kernel, parts, members), out_sha...  293 us
    all_gather x2, blocking collectives, sum_over_hidden(): return lax.all_gather(summed, 'fs', axis=1, tiled=True).astype(jnp.float32)  66.5 us
    all_to_all x2, waiting for transfers between devices, sum_over_hidden(): lax.all_to_all(partial_value.astype(jnp.bfloat16), 'fs', split_axis=1, co...  50.9 us
    all_gather x1, waiting for transfers between devices, on_device(): lax.all_gather(down_second.astype(jnp.bfloat16), 'tp', axis=1, tiled=True)  38.6 us
    all_to_all x2, starting transfers between devices, sum_over_hidden(): lax.all_to_all(partial_value.astype(jnp.bfloat16), 'fs', split_axis=1, co...  18.6 us
    dot_general x2, matrix products, hidden_part(): return jnp.dot(hidden, w_down, preferred_element_type=jnp.float32)  15.4 us
    transpose x2, local copies, waits for them, and re-layouts, ordered(): return split.transpose(1, 0, 2, 3).reshape(members * rows, owned)  13.4 us
  transfers between devices with their start and end apart: 8, of which 4 were waited for; matrix products, arithmetic and copies ran while one was open for 8% of the time, Pallas kernels for 40%

profile of v3, /device:TPU:0, one launch (start us, length us, event | category | flops | bytes accessed | tf_op | source)
XLA Modules:
  0.0 558.5 jit_solution(3858786053781457962)
XLA Ops:
  7.2 3.3 convert_element_type.63
  10.7 4.5 multiply_convert_fusion.1
  15.1 67.6 %scatter_pieces.4 = bf16[768,1024]{1,0:T(8,128)(2,1)} custom-call(bf16[384,2048]{1,0:T(8,128)(2,1)} %get-tuple-element.20.source), custom_call_target="tpu_custom_call" | custom-call | bytes 100663296 | tf_op jit(solution)/shard_map/scatter_pieces/pallas_call | solution.py:78
  82.8 75.0 %scatter_pieces.5 = bf16[768,1024]{1,0:T(8,128)(2,1)} custom-call(bf16[384,2048]{1,0:T(8,128)(2,1)} %get-tuple-element.21.source), custom_call_target="tpu_custom_call" | custom-call | bytes 100663296 | tf_op jit(solution)/shard_map/scatter_pieces/pallas_call | solution.py:78
  157.9 4.5 multiply_convert_fusion.2
  162.5 0.7 all-gather.11.cloned.1.call-update
  163.2 75.0 %scatter_pieces.6 = bf16[768,1024]{1,0:T(8,128)(2,1)} custom-call(bf16[384,2048]{1,0:T(8,128)(2,1)} %get-tuple-element.22.source), custom_call_target="tpu_custom_call" | custom-call | bytes 100663296 | tf_op jit(solution)/shard_map/scatter_pieces/pallas_call | solution.py:78
  238.2 75.0 %scatter_pieces.7 = bf16[768,1024]{1,0:T(8,128)(2,1)} custom-call(bf16[384,2048]{1,0:T(8,128)(2,1)} %get-tuple-element.23.source), custom_call_target="tpu_custom_call" | custom-call | bytes 100663296 | tf_op jit(solution)/shard_map/scatter_pieces/pallas_call | solution.py:78
  314.9 3.2 convert_element_type.72
  318.1 6.6 %copy.20 = bf16[8,4,96,1024]{3,2,1,0:T(8,128)(2,1)} copy(bf16[8,4,96,1024]{3,2,0,1:T(8,128)(2,1)} %bitcast.45) | data formatting | bytes 12582912 | tf_op jit(solution)/shard_map/transpose | solution.py:103
  324.8 6.8 %copy.21 = bf16[8,4,96,1024]{3,2,1,0:T(8,128)(2,1)} copy(bf16[8,4,96,1024]{3,2,0,1:T(8,128)(2,1)} %bitcast.47) | data formatting | bytes 12582912 | tf_op jit(solution)/shard_map/transpose | solution.py:103
  331.6 1.3 fusion.12
  332.9 8.5 %convolution_convert_fusion.1 = bf16[160,3072]{1,0:T(8,128)(2,1)S(1)} fusion(bf16[1024,3072]{1,0:T(8,128)(2,1)} %all-gather.11.cloned.1.call-done, bf16[160,3072]{1,0:T(8,128)(2,1)S(1)} %fusion.3, bf16[3072,1024]{1,0:T(8,128)(2,1)} %bitcast.42, f32[160,1024]{1,0:T(8,128)S(1)} %fusion.12), kind=kOutput, calls=%fused_computation.1 | convolution fusion | flops 2014740480 | bytes 15204352 | tf_op jit(solution)/shard_map/dot_general | solution.py:137
  341.4 1.0 copy.31
  342.5 13.1 %all-to-all-start = ((bf16[160,8,384]{2,0,1:T(8,128)(2,1)}), bf16[160,8,384]{2,0,1:T(8,128)(2,1)S(1)}, u32[]{:S(2)}, u32[]{:S(2)}) async-start(bf16[160,8,384]{2,0,1:T(8,128)(2,1)} %bitcast.35), calls=%async_computation | async-start | bytes 1966080 | tf_op jit(solution)/shard_map/all_to_all | solution.py:114
  355.6 26.2 %all-to-all-done = bf16[160,8,384]{2,0,1:T(8,128)(2,1)S(1)} async-done(((bf16[160,8,384]{2,0,1:T(8,128)(2,1)}), bf16[160,8,384]{2,0,1:T(8,128)(2,1)S(1)}, u32[]{:S(2)}, u32[]{:S(2)}) %all-to-all-start) | async-done | bytes 983072 | tf_op jit(solution)/shard_map/all_to_all | solution.py:114
  381.9 33.5 %all_gather.41 = bf16[160,3072]{1,0:T(8,128)(2,1)S(1)} all-gather(bf16[160,384]{1,0:T(8,128)(2,1)S(1)} %reduce_sum.80), channel_id=1, replica_groups=mesh['fs'=8,'tp'=4] {'fs'}, dimensions={1}, use_global_device_ids=true | all-gather | bytes 1105920 | tf_op jit(solution)/shard_map/all_gather | solution.py:120
  415.9 0.6 multiply_reduce_fusion.1
  417.1 3.4 all-gather.19.cloned.1.call-done
  420.5 3.7 copy.23
  424.2 0.9 copy-done.3
  425.1 3.9 copy.24
  429.0 1.3 fusion.13
  430.3 38.6 %all-gather.13.cloned.1.call-done = bf16[1024,3072]{1,0:T(8,128)(2,1)} async-done(((bf16[1024,768]{1,0:T(8,128)(2,1)}), bf16[1024,3072]{1,0:T(8,128)(2,1)}) %all-gather.13.cloned.1.call-update) | async-done | bytes 6291472 | tf_op jit(solution)/shard_map/all_gather | solution.py:174
  468.9 6.9 %convolution_convert_fusion = bf16[160,3072]{1,0:T(8,128)(2,1)S(1)} fusion(bf16[1024,3072]{1,0:T(8,128)(2,1)} %all-gather.13.cloned.1.call-done, bf16[160,3072]{1,0:T(8,128)(2,1)S(1)} %multiply_convert_fusion.5, bf16[3072,1024]{1,0:T(8,128)(2,1)} %bitcast.48, f32[160,1024]{1,0:T(8,128)S(1)} %fusion.13), kind=kOutput, calls=%fused_computation | convolution fusion | flops 2014740480 | bytes 15204352 | tf_op jit(solution)/shard_map/dot_general | solution.py:137
  475.8 1.0 copy.30
  476.8 5.5 all-to-all-start.1
  482.4 24.8 %all-to-all-done.1 = bf16[160,8,384]{2,0,1:T(8,128)(2,1)S(1)} async-done(((bf16[160,8,384]{2,0,1:T(8,128)(2,1)}), bf16[160,8,384]{2,0,1:T(8,128)(2,1)S(1)}, u32[]{:S(2)}, u32[]{:S(2)}) %all-to-all-start.1) | async-done | bytes 983072 | tf_op jit(solution)/shard_map/all_to_all | solution.py:114
  507.3 33.0 %all_gather.47 = bf16[160,3072]{1,0:T(8,128)(2,1)S(1)} all-gather(bf16[160,384]{1,0:T(8,128)(2,1)S(1)} %reduce_sum.83), channel_id=1, replica_groups=mesh['fs'=8,'tp'=4] {'fs'}, dimensions={1}, use_global_device_ids=true | all-gather | bytes 1105920 | tf_op jit(solution)/shard_map/all_gather | solution.py:120
  541.4 1.5 multiply_convert_fusion.4
  542.9 6.1 %copy.34 = bf16[1024,3072]{1,0:T(8,128)(2,1)} copy(bf16[1024,3072]{1,0:T(8,128)(2,1)} %all-gather.11.cloned.1.call-done) | data formatting | bytes 12582912
  548.9 2.7 copy.35
  (54 shorter events, 4.5 us)
Async XLA Ops:
  7.2 311.0 %all-gather.15.cloned.1.call-start = ((), (), s32[]{:S(2)}) async-start(), calls=%async_computation.4 | async-start | bytes 7864320 | tf_op jit(solution)/shard_map/all_gather | solution.py:96
  7.2 3.4 copy-start.6
  7.2 3.4 copy-start.4
  82.7 75.1 %copy-start.7 = (f32[3072]{0:T(1024)S(1)}, f32[3072]{0:T(1024)}, u32[]{:S(2)}) copy-start(f32[3072]{0:T(1024)} %param.11) | copy-start | bytes 36868
  82.8 75.2 %copy-start.5 = (f32[384,2048]{1,0:T(8,128)S(1)}, f32[384,2048]{1,0:T(8,128)}, u32[]{:S(2)}) copy-start(f32[384,2048]{1,0:T(8,128)} %param.15) | copy-start | bytes 9437188
  82.8 242.0 %all-gather.17.cloned.1.call-start = ((), (), s32[]{:S(2)}) async-start(), calls=%async_computation.5 | async-start | bytes 7864320 | tf_op jit(solution)/shard_map/all_gather | solution.py:96
  162.4 170.4 %all-gather.11.cloned.1.call-start = ((), (), s32[]{:S(2)}) async-start(), calls=%async_computation.2 | async-start | bytes 7864320 | tf_op jit(solution)/shard_map/all_gather | solution.py:173
  163.2 253.9 %all-gather.21.cloned.1.call-start = ((), (), s32[]{:S(2)}) async-start(), calls=%async_computation.7 | async-start | bytes 7864320 | tf_op jit(solution)/shard_map/all_gather | solution.py:186
  238.2 75.0 %copy-start.2 = (bf16[160,3072]{1,0:T(8,128)(2,1)S(1)}, bf16[160,3072]{1,0:T(8,128)(2,1)}, u32[]{:S(2)}) copy-start(bf16[160,3072]{1,0:T(8,128)(2,1)} %param.9) | copy-start | bytes 2949124
  314.3 106.3 %all-gather.19.cloned.1.call-start = ((), (), s32[]{:S(2)}) async-start(), calls=%async_computation.6 | async-start | bytes 7864320 | tf_op jit(solution)/shard_map/all_gather | solution.py:186
  314.9 154.0 %all-gather.13.cloned.1.call-start = ((), (), s32[]{:S(2)}) async-start(), calls=%async_computation.3 | async-start | bytes 7864320 | tf_op jit(solution)/shard_map/all_gather | solution.py:174
  324.8 6.8 %copy-start = (bf16[8,4,96,1024]{3,2,1,0:T(8,128)(2,1)S(1)}, bf16[8,4,96,1024]{3,2,1,0:T(8,128)(2,1)}, u32[]{:S(2)}) copy-start(bf16[8,4,96,1024]{3,2,1,0:T(8,128)(2,1)} %copy.20) | copy-start | bytes 18874372
  342.5 39.3 %all-to-all-start = ((bf16[160,8,384]{2,0,1:T(8,128)(2,1)}), bf16[160,8,384]{2,0,1:T(8,128)(2,1)S(1)}, u32[]{:S(2)}, u32[]{:S(2)}) async-start(bf16[160,8,384]{2,0,1:T(8,128)(2,1)} %bitcast.35), calls=%async_computation | async-start | bytes 1966080 | tf_op jit(solution)/shard_map/all_to_all | solution.py:114
  420.5 4.6 copy-start.3
  424.2 4.8 copy-start.1
  476.8 30.3 %all-to-all-start.1 = ((bf16[160,8,384]{2,0,1:T(8,128)(2,1)}), bf16[160,8,384]{2,0,1:T(8,128)(2,1)S(1)}, u32[]{:S(2)}, u32[]{:S(2)}) async-start(bf16[160,8,384]{2,0,1:T(8,128)(2,1)} %bitcast.34), calls=%async_computation.1 | async-start | bytes 1966080 | tf_op jit(solution)/shard_map/all_to_all | solution.py:114
  541.4 7.6 %slice-start = ((s8[6291456]{0:T(1024)(128)(4,1)}), s8[4194304]{0:T(1024)(128)(4,1)S(1)}, s32[]{:S(2)}) async-start(s8[6291456]{0:T(1024)(128)(4,1)} %bitcast.40), calls=%async_computation.8 | async-start | bytes 8388608
  542.8 6.1 %slice-start.1 = ((s8[6291456]{0:T(1024)(128)(4,1)}), s8[2097152]{0:T(1024)(128)(4,1)S(1)}, s32[]{:S(2)}) async-start(s8[6291456]{0:T(1024)(128)(4,1)} %bitcast.40), calls=%async_computation.9 | async-start | bytes 4194304
Sparse Core Ops, SparseCore 0:
  82.9 80.9 all-gather.14
  165.4 78.7 all-gather.16
  246.4 72.8 all-gather.10
  320.7 52.0 all-gather.20
  374.1 46.3 all-gather.18
  422.5 46.3 all-gather.12
